TPU v7x, 512 devices: a whole 4x8x8 slice. The times are simulated.
512 devices in a mesh: dp: 4 (over x), kv: 64 (over z, y), tp: 2 (over core).
Axes of the slice: x: 4, y: 8, z: 8, core: 2. Of those that a mesh axis runs over, the one named last changes fastest.
Arguments:
- tokens: bfloat16 [256, 4096], P('dp', ('kv', 'tp')), parts along dimension 0, may hold values from -16 to 16
- mix_gain: float32 [4096], replicated, may hold values from 0.1 to 1.9
- w_query: bfloat16 [4096, 2048], P('kv', 'tp'), may hold values from -0.09375 to 0.09375
- w_key: bfloat16 [4096, 2048], P('kv', 'tp'), may hold values from -0.09375 to 0.09375
- w_value: bfloat16 [4096, 4096], P('kv', 'tp'), may hold values from -0.09375 to 0.09375
- w_igate: bfloat16 [4096, 16], replicated, may hold values from -0.09375 to 0.09375
- w_fgate: bfloat16 [4096, 16], replicated, may hold values from -0.09375 to 0.09375
- igate_bias: float32 [16], replicated, may hold values from -3 to 1
- fgate_bias: float32 [16], replicated, may hold values from -2 to 5
- memory: float32 [256, 16, 256, 128], P(('dp', 'kv'), 'tp'), parts along dimension 0, may hold values from -6 to 6
- normalizer: float32 [256, 16, 128], P(('dp', 'kv'), 'tp'), parts along dimension 0, may hold values from -6 to 6
- stabilizer: float32 [256, 16], P(('dp', 'kv'), 'tp'), parts along dimension 0, may hold values from -3 to 3
- w_output: bfloat16 [4096, 4096], P('tp', 'kv'), may hold values from -0.09375 to 0.09375
- mlp_gain: float32 [4096], replicated, may hold values from 0.1 to 1.9
- w_up: bfloat16 [4096, 16384], P(None, ('kv', 'tp')), may hold values from -0.09375 to 0.09375
- w_down: bfloat16 [16384, 4096], P(('kv', 'tp')), may hold values from -0.1875 to 0.1875
Outputs:
- new_tokens: bfloat16 [256, 4096], P('dp', ('kv', 'tp')), parts along dimension 0
- new_memory: float32 [256, 16, 256, 128], P(('dp', 'kv'), 'tp'), parts along dimension 0
- new_normalizer: float32 [256, 16, 128], P(('dp', 'kv'), 'tp'), parts along dimension 0
- new_stabilizer: float32 [256, 16], P(('dp', 'kv'), 'tp'), parts along dimension 0
There are 4 independent parts, one for each index of `dp`. A program takes and returns all parts, laid end to end along the dimension named above; an argument that names none is the same for every part. Nothing has to cross between parts.
All inputs are finite; a program needn't handle non-finite values.
Results may differ from a plain program's by a relative error of at most 0.019.
Values may be sent and summed in bfloat16 or wider, within the bound.
No kernel may reach another device: no remote copies, remote signals or barrier semaphores. Data moves between devices by JAX's collectives and lax.ppermute only.
A program may use at most 64 MiB of HBM per device.

v0:
```python
import jax
import jax.numpy as jnp
from jax import lax
from jax.sharding import PartitionSpec as P

DV = 256
DQK = 128
norm_eps = 1e-06


def cut_along(shard, dim, length):
    before, after = (shard.shape[:dim], shard.shape[dim + 1 :])
    return jnp.moveaxis(shard.reshape(*before, length, -1, *after), dim, 0)


def summed_on_arrival(shard, axis, dim):
    length = lax.axis_size(axis)
    tiles = lax.all_to_all(cut_along(shard, dim, length), axis, 0, 0, tiled=True)
    return jnp.sum(tiles.astype(jnp.float32), axis=0)


def from_everyone(shard, axis):
    length = lax.axis_size(axis)
    return lax.all_to_all(
        jnp.broadcast_to(shard[None], (length, *shard.shape)), axis, 0, 0, tiled=True
    )


def joined_along(tiles, dim):
    dims = list(tiles.shape[1:])
    dims[dim] *= tiles.shape[0]
    return jnp.moveaxis(tiles, 0, dim).reshape(dims)


def collect(shard, axis, dim):
    tiles = from_everyone(shard, axis)
    return joined_along(tiles, dim)


def of_everyone(shard, axis):
    return from_everyone(shard, axis).astype(jnp.float32).sum(axis=0)


def rms_normed(rows, gain):
    wide_rows = rows.astype(jnp.float32)
    scale = lax.rsqrt(jnp.mean(wide_rows * wide_rows, axis=-1, keepdims=True) + norm_eps)
    return (wide_rows * scale * gain).astype(jnp.bfloat16)


def on_device(
    tokens,
    mix_gain,
    w_query,
    w_key,
    w_value,
    w_igate,
    w_fgate,
    igate_bias,
    fgate_bias,
    memory,
    normalizer,
    stabilizer,
    w_output,
    mlp_gain,
    w_up,
    w_down,
):
    kv_count = lax.axis_size("kv")
    tp_count = lax.axis_size("tp")
    kv_index = lax.axis_index("kv")
    tp_index = lax.axis_index("tp")
    own_rows = memory.shape[0]
    head_count = memory.shape[1]
    whole_rows = lax.all_gather(tokens, ("kv", "tp"), axis=1, tiled=True)
    wide_rows = whole_rows.astype(jnp.float32)
    normed = rms_normed(whole_rows, mix_gain)
    row_span = w_query.shape[0]
    own_cols = lax.dynamic_slice_in_dim(normed, kv_index * row_span, row_span, 1)
    joined = summed_on_arrival(
        jnp.concatenate(
            [
                jnp.dot(own_cols, w_query, preferred_element_type=jnp.float32),
                jnp.dot(own_cols, w_key, preferred_element_type=jnp.float32),
                jnp.dot(own_cols, w_value, preferred_element_type=jnp.float32),
            ],
            axis=1,
        ).astype(jnp.bfloat16),
        "kv",
        0,
    )
    query_cols = w_query.shape[1]
    queries = joined[:, :query_cols].reshape(own_rows, head_count, DQK) * DQK ** (-0.5)
    key_rows = joined[:, query_cols : 2 * query_cols].reshape(own_rows, head_count, DQK)
    values = joined[:, 2 * query_cols :].reshape(own_rows, head_count, DV)
    own_normed = lax.dynamic_slice_in_dim(normed, kv_index * own_rows, own_rows, 0)
    igate_cols = lax.dynamic_slice_in_dim(w_igate, tp_index * head_count, head_count, 1)
    fgate_cols = lax.dynamic_slice_in_dim(w_fgate, tp_index * head_count, head_count, 1)
    ibias_own = lax.dynamic_slice_in_dim(igate_bias, tp_index * head_count, head_count, 0)
    fbias_own = lax.dynamic_slice_in_dim(fgate_bias, tp_index * head_count, head_count, 0)
    input_gate = jnp.dot(own_normed, igate_cols, preferred_element_type=jnp.float32) + ibias_own
    log_forget = jax.nn.log_sigmoid(
        jnp.dot(own_normed, fgate_cols, preferred_element_type=jnp.float32) + fbias_own
    )
    carried = log_forget + stabilizer
    new_stabilizer = jnp.maximum(carried, input_gate)
    keep_weight = jnp.exp(carried - new_stabilizer)
    fresh_weight = jnp.exp(input_gate - new_stabilizer)
    recall = jnp.einsum("bhvd,bhd->bhv", memory, queries, precision=lax.Precision.HIGHEST)
    match_score = jnp.sum(queries * key_rows, axis=-1)
    numerator = keep_weight[..., None] * recall + (fresh_weight * match_score)[..., None] * values
    denominator = keep_weight * jnp.sum(normalizer * queries, axis=-1) + fresh_weight * match_score
    floor_value = jnp.maximum(jnp.abs(denominator), jnp.exp(-new_stabilizer))
    cell_out = (
        (numerator / floor_value[..., None]).astype(jnp.bfloat16).reshape(own_rows, head_count * DV)
    )
    new_memory = (
        keep_weight[..., None, None] * memory
        + fresh_weight[..., None, None] * values[..., :, None] * key_rows[..., None, :]
    )
    new_normalizer = keep_weight[..., None] * normalizer + fresh_weight[..., None] * key_rows
    partial_value = jnp.dot(
        collect(cell_out, "kv", 0), w_output, preferred_element_type=jnp.float32
    )
    block_cols = partial_value.shape[1]
    pair_total = of_everyone(partial_value.astype(jnp.bfloat16), "tp").astype(jnp.float32)
    local_rows = lax.dynamic_slice_in_dim(wide_rows, kv_index * block_cols, block_cols, 1)
    middle_block = (local_rows + pair_total).astype(jnp.bfloat16)
    middle = collect(middle_block, "kv", 1)
    mixer_in = rms_normed(middle, mlp_gain)
    up_rows = jnp.dot(mixer_in, w_up, preferred_element_type=jnp.float32)
    activation = jnp.square(jax.nn.relu(up_rows)).astype(jnp.bfloat16)
    thin_cols = tokens.shape[1]
    hidden_rows = w_down.shape[0]
    reordered = jnp.transpose(
        w_down.reshape(hidden_rows, kv_count, tp_count, thin_cols), (0, 2, 1, 3)
    ).reshape(hidden_rows, tp_count * kv_count * thin_cols)
    chip_sums = summed_on_arrival(
        lax.dot_general(
            reordered, activation, (((0,), (1,)), ((), ())), preferred_element_type=jnp.float32
        ).astype(jnp.bfloat16),
        "tp",
        0,
    )
    down_cols = summed_on_arrival(chip_sums.astype(jnp.bfloat16), "kv", 0)
    middle_own = lax.dynamic_slice_in_dim(
        middle, (kv_index * tp_count + tp_index) * thin_cols, thin_cols, 1
    )
    new_tokens = (middle_own.astype(jnp.float32) + down_cols.T).astype(jnp.bfloat16)
    return (new_tokens, new_memory, new_normalizer, new_stabilizer)


def solution(mesh):
    in_specs = (
        P("dp", ("kv", "tp")),
        P(),
        P("kv", "tp"),
        P("kv", "tp"),
        P("kv", "tp"),
        P(),
        P(),
        P(),
        P(),
        P(("dp", "kv"), "tp", None, None),
        P(("dp", "kv"), "tp", None),
        P(("dp", "kv"), "tp"),
        P("tp", "kv"),
        P(),
        P(None, ("kv", "tp")),
        P(("kv", "tp"), None),
    )
    out_specs = (
        P("dp", ("kv", "tp")),
        P(("dp", "kv"), "tp", None, None),
        P(("dp", "kv"), "tp", None),
        P(("dp", "kv"), "tp"),
    )
    return jax.shard_map(
        on_device, mesh=mesh, in_specs=in_specs, out_specs=out_specs, check_vma=False
    )
```

profile of v0, /device:TPU:4, one launch (start us, length us, event | category | flops | bytes accessed | tf_op | source)
XLA Modules:
  0.0 191.2 jit_solution(15945729594412308125)
XLA Ops:
  0.6 0.0 copy-start
  0.6 58.2 %all_gather.3 = bf16[64,4096]{0,1:T(8,128)(2,1)S(1)} all-gather(bf16[64,32]{0,1:T(8,128)(2,1)} %param.16), channel_id=1, replica_groups=mesh['dp'=4,'kv'=64,'tp'=2] {'kv','tp'}, dimensions={1}, use_global_device_ids=true | all-gather | bytes 528384 | tf_op jit(solution)/shard_map/all_gather | solution.py:74
  58.9 0.3 copy.41
  59.2 0.0 copy-start.3
  59.2 0.0 copy-start.4
  59.2 0.2 multiply_reduce_fusion.1
  59.5 0.1 copy-done.6
  59.6 0.2 multiply_convert_fusion.3
  59.8 0.4 copy-done.3
  60.1 0.3 fusion
  60.4 0.2 fusion.2
  60.7 0.2 fusion.1
  61.0 0.5 broadcast.126
  61.5 1.0 reduce.9
  62.5 0.0 copy-start.11
  62.5 0.0 copy-start.13
  62.5 0.0 copy-start.12
  62.5 0.0 copy-start.14
  62.5 0.0 copy-start.15
  62.6 1.2 reshape.279
  63.7 7.4 %all-to-all-start = ((bf16[64,2,2048]{2,1,0:T(2,128)(2,1)}), bf16[64,2,2048]{2,1,0:T(2,128)(2,1)S(1)}, u32[]{:S(2)}, u32[]{:S(2)}) async-start(bf16[64,2,2048]{2,1,0:T(2,128)(2,1)} %reshape.279), calls=%async_computation | async-start | bytes 1048576 | tf_op jit(solution)/shard_map/all_to_all | solution.py:18
  71.2 1.0 fusion.8
  72.2 1.0 bitcast_add_fusion.1
  73.2 0.0 copy-start.9
  73.3 17.3 %all-to-all-done = bf16[64,2,2048]{2,1,0:T(2,128)(2,1)S(1)} async-done(((bf16[64,2,2048]{2,1,0:T(2,128)(2,1)}), bf16[64,2,2048]{2,1,0:T(2,128)(2,1)S(1)}, u32[]{:S(2)}, u32[]{:S(2)}) %all-to-all-start) | async-done | bytes 524320 | tf_op jit(solution)/shard_map/all_to_all | solution.py:18
  90.6 1.8 reshape.280
  92.3 2.4 %convert_reduce_fusion.1 = f32[4096]{0:T(1024)S(1)} fusion(bf16[64,1,4096]{2,1,0:T(2,128)(2,1)} %reshape.280), kind=kLoop, calls=%fused_computation.25 | loop fusion | flops 520192 | bytes 540672 | tf_op jit(solution)/shard_map/reduce_sum | solution.py:19
  94.8 1.0 fusion.9
  95.7 0.8 multiply_reduce_fusion.3
  96.6 0.1 broadcast_multiply_fusion
  96.7 0.3 broadcast_in_dim.9
  97.0 2.2 %reduce.10 = bf16[64,2048]{1,0:T(8,128)(2,1)S(1)} reduce(bf16[64,1,2048]{2,1,0:T(2,128)(2,1)S(1)} %broadcast_in_dim.9, bf16[]{:T(256)} %broadcast.126), dimensions={1}, to_apply=%broadcast_in_dim.9.reduce_sub_computation | reduce | bytes 524290 | tf_op jit(solution)/shard_map/broadcast_in_dim | solution.py:25
  99.1 0.9 reshape.281
  100.0 6.0 %all-to-all-start.1 = ((bf16[64,2,1024]{2,1,0:T(2,128)(2,1)}), bf16[64,2,1024]{2,1,0:T(2,128)(2,1)S(1)}, u32[]{:S(2)}, u32[]{:S(2)}) async-start(bf16[64,2,1024]{2,1,0:T(2,128)(2,1)} %reshape.281), calls=%async_computation.1 | async-start | bytes 524288 | tf_op jit(solution)/shard_map/all_to_all | solution.py:24
  106.0 0.0 copy-start.10
  106.0 1.0 convert_element_type.60
  107.1 13.3 %all-to-all-done.1 = bf16[64,2,1024]{2,1,0:T(2,128)(2,1)S(1)} async-done(((bf16[64,2,1024]{2,1,0:T(2,128)(2,1)}), bf16[64,2,1024]{2,1,0:T(2,128)(2,1)S(1)}, u32[]{:S(2)}, u32[]{:S(2)}) %all-to-all-start.1) | async-done | bytes 262176 | tf_op jit(solution)/shard_map/all_to_all | solution.py:24
  120.4 0.2 reshape.282
  120.6 0.3 convolution_convert_fusion.4
  120.9 0.1 reshape.283
  121.0 3.7 %all_to_all.30 = bf16[2,2,2048]{2,1,0:T(2,128)(2,1)S(1)} all-to-all(bf16[2,2,2048]{2,1,0:T(2,128)(2,1)S(1)} %reshape.283), channel_id=1, replica_groups=mesh['dp'=4,'kv'=64,'tp'=2] {'tp'}, dimensions={0} | all-to-all | bytes 32768 | tf_op jit(solution)/shard_map/all_to_all | solution.py:24
  124.7 0.1 reshape.284
  124.9 0.8 add_convert_fusion
  125.7 0.1 copy.43
  125.8 0.3 broadcast_bitcast_fusion
  126.1 1.6 reshape.285
  127.6 5.5 %all-to-all-start.3 = ((bf16[64,2,2048]{2,1,0:T(2,128)(2,1)}), bf16[64,2,2048]{2,1,0:T(2,128)(2,1)}, u32[]{:S(2)}, u32[]{:S(2)}) async-start(bf16[64,2,2048]{2,1,0:T(2,128)(2,1)} %reshape.285), calls=%async_computation.3 | async-start | bytes 1048576 | tf_op jit(solution)/shard_map/all_to_all | solution.py:24
  133.1 1.6 copy.44
  134.7 1.1 copy.45
  135.8 16.3 %all-to-all-done.3 = bf16[64,2,2048]{2,1,0:T(2,128)(2,1)} async-done(((bf16[64,2,2048]{2,1,0:T(2,128)(2,1)}), bf16[64,2,2048]{2,1,0:T(2,128)(2,1)}, u32[]{:S(2)}, u32[]{:S(2)}) %all-to-all-start.3) | async-done | bytes 524320 | tf_op jit(solution)/shard_map/all_to_all | solution.py:24
  152.1 2.3 %reshape.286 = bf16[64,64,64]{2,1,0:T(8,128)(2,1)S(1)} reshape(bf16[64,2,2048]{2,1,0:T(2,128)(2,1)} %all-to-all-done.3) | data formatting | bytes 1048576
  154.4 0.6 multiply_reduce_fusion
  154.9 3.5 %convolution_convert_fusion = bf16[64,4096]{1,0:T(8,128)(2,1)} fusion(bf16[128,4096]{0,1:T(8,128)(2,1)} %bitcast.116, bf16[4096,128]{1,0:T(8,128)(2,1)S(1)} %copy-done, bf16[64,4096]{0,1:T(8,128)(2,1)S(1)} %bitcast.113, f32[4096]{0:T(1024)S(1)} %copy-done.7, f32[64]{0:T(128)S(1)} %add_rsqrt_fusion), kind=kOutput, calls=%fused_computation | convolution fusion | flops 135553024 | bytes 3162368 | tf_op jit(solution)/shard_map/dot_general | solution.py:138
  158.4 1.1 copy.63
  159.5 4.9 %all_to_all.31 = bf16[2,2048,64]{1,2,0:T(8,128)(2,1)} all-to-all(bf16[2,2048,64]{1,2,0:T(8,128)(2,1)S(1)} %bitcast.118), channel_id=1, replica_groups=mesh['dp'=4,'kv'=64,'tp'=2] {'tp'}, dimensions={0} | all-to-all | bytes 1048576 | tf_op jit(solution)/shard_map/all_to_all | solution.py:18
  164.4 1.1 reduce_sum.90
  165.6 1.0 copy.48
  166.6 2.1 %reshape.287 = bf16[64,2,1024]{2,1,0:T(2,128)(2,1)} reshape(bf16[64,32,64]{2,1,0:T(8,128)(2,1)} %bitcast.117) | data formatting | bytes 524288
  168.6 6.2 %all-to-all-start.5 = ((bf16[64,2,1024]{2,1,0:T(2,128)(2,1)}), bf16[64,2,1024]{2,1,0:T(2,128)(2,1)S(1)}, u32[]{:S(2)}, u32[]{:S(2)}) async-start(bf16[64,2,1024]{2,1,0:T(2,128)(2,1)} %reshape.287), calls=%async_computation.5 | async-start | bytes 524288 | tf_op jit(solution)/shard_map/all_to_all | solution.py:18
  174.9 1.3 multiply_add_fusion
  176.2 13.9 %all-to-all-done.5 = bf16[64,2,1024]{2,1,0:T(2,128)(2,1)S(1)} async-done(((bf16[64,2,1024]{2,1,0:T(2,128)(2,1)}), bf16[64,2,1024]{2,1,0:T(2,128)(2,1)S(1)}, u32[]{:S(2)}, u32[]{:S(2)}) %all-to-all-start.5) | async-done | bytes 262176 | tf_op jit(solution)/shard_map/all_to_all | solution.py:18
  190.1 0.3 reshape.288
  190.4 0.1 convert_reduce_fusion
  190.5 0.6 fusion.21
  (32 shorter events, 0.2 us)
Async XLA Ops:
  0.6 154.3 %copy-start = (bf16[4096,128]{1,0:T(8,128)(2,1)S(1)}, bf16[4096,128]{1,0:T(8,128)(2,1)}, u32[]{:S(2)}) copy-start(bf16[4096,128]{1,0:T(8,128)(2,1)} %param.30) | copy-start | bytes 3145732
  58.9 0.7 copy-start.6
  59.2 1.0 copy-start.3
  59.2 1.2 copy-start.4
  59.4 1.3 copy-start.5
  59.8 0.9 copy-start.2
  62.5 8.7 %copy-start.11 = (bf16[4096,16]{0,1:T(8,128)(2,1)S(1)}, bf16[4096,16]{0,1:T(8,128)(2,1)}, u32[]{:S(2)}) copy-start(bf16[4096,16]{0,1:T(8,128)(2,1)} %param.21) | copy-start | bytes 393220
  62.5 8.7 %copy-start.13 = (f32[16]{0:T(128)S(1)}, f32[16]{0:T(128)}, u32[]{:S(2)}) copy-start(f32[16]{0:T(128)} %param.23) | copy-start | bytes 196
  62.5 9.7 %copy-start.12 = (bf16[4096,16]{0,1:T(8,128)(2,1)S(1)}, bf16[4096,16]{0,1:T(8,128)(2,1)}, u32[]{:S(2)}) copy-start(bf16[4096,16]{0,1:T(8,128)(2,1)} %param.22) | copy-start | bytes 393220
  62.5 9.7 %copy-start.14 = (f32[1,8]{1,0:T(1,128)S(1)}, f32[1,8]{1,0:T(1,128)}, u32[]{:S(2)}) copy-start(f32[1,8]{1,0:T(1,128)} %param.27) | copy-start | bytes 100
  62.5 9.6 %copy-start.15 = (f32[16]{0:T(128)S(1)}, f32[16]{0:T(128)}, u32[]{:S(2)}) copy-start(f32[16]{0:T(128)} %param.24) | copy-start | bytes 196
  63.7 26.8 %all-to-all-start = ((bf16[64,2,2048]{2,1,0:T(2,128)(2,1)}), bf16[64,2,2048]{2,1,0:T(2,128)(2,1)S(1)}, u32[]{:S(2)}, u32[]{:S(2)}) async-start(bf16[64,2,2048]{2,1,0:T(2,128)(2,1)} %reshape.279), calls=%async_computation | async-start | bytes 1048576 | tf_op jit(solution)/shard_map/all_to_all | solution.py:18
  73.2 23.3 %copy-start.9 = (f32[1,8]{1,0:T(1,128)}, f32[1,8]{1,0:T(1,128)S(1)}, u32[]{:S(2)}) copy-start(f32[1,8]{1,0:T(1,128)S(1)} %get-tuple-element.7) | copy-start | bytes 100
  73.2 21.5 %copy-start.1 = (f32[1,8,256,128]{3,2,1,0:T(8,128)S(1)}, f32[1,8,256,128]{3,2,1,0:T(8,128)}, u32[]{:S(2)}) copy-start(f32[1,8,256,128]{3,2,1,0:T(8,128)} %param.25) | copy-start | bytes 3145732
  92.3 3.4 %copy-start.8 = (f32[1,8,128]{2,1,0:T(8,128)S(1)}, f32[1,8,128]{2,1,0:T(8,128)}, u32[]{:S(2)}) copy-start(f32[1,8,128]{2,1,0:T(8,128)} %param.26) | copy-start | bytes 12292
  100.0 20.4 %all-to-all-start.1 = ((bf16[64,2,1024]{2,1,0:T(2,128)(2,1)}), bf16[64,2,1024]{2,1,0:T(2,128)(2,1)S(1)}, u32[]{:S(2)}, u32[]{:S(2)}) async-start(bf16[64,2,1024]{2,1,0:T(2,128)(2,1)} %reshape.281), calls=%async_computation.1 | async-start | bytes 524288 | tf_op jit(solution)/shard_map/all_to_all | solution.py:24
  106.0 14.6 %copy-start.10 = (bf16[2048,64]{0,1:T(8,128)(2,1)S(1)}, bf16[2048,64]{0,1:T(8,128)(2,1)}, u32[]{:S(2)}) copy-start(bf16[2048,64]{0,1:T(8,128)(2,1)} %param.28) | copy-start | bytes 786436
  127.6 24.5 %all-to-all-start.3 = ((bf16[64,2,2048]{2,1,0:T(2,128)(2,1)}), bf16[64,2,2048]{2,1,0:T(2,128)(2,1)}, u32[]{:S(2)}, u32[]{:S(2)}) async-start(bf16[64,2,2048]{2,1,0:T(2,128)(2,1)} %reshape.285), calls=%async_computation.3 | async-start | bytes 1048576 | tf_op jit(solution)/shard_map/all_to_all | solution.py:24
  135.8 19.1 %copy-start.7 = (f32[4096]{0:T(1024)S(1)}, f32[4096]{0:T(1024)}, u32[]{:S(2)}) copy-start(f32[4096]{0:T(1024)} %param.29) | copy-start | bytes 49156
  168.6 21.4 %all-to-all-start.5 = ((bf16[64,2,1024]{2,1,0:T(2,128)(2,1)}), bf16[64,2,1024]{2,1,0:T(2,128)(2,1)S(1)}, u32[]{:S(2)}, u32[]{:S(2)}) async-start(bf16[64,2,1024]{2,1,0:T(2,128)(2,1)} %reshape.287), calls=%async_computation.5 | async-start | bytes 524288 | tf_op jit(solution)/shard_map/all_to_all | solution.py:18
where the time goes:
time: 192 us; the launch traced here: 191 us
  blocking collectives  66.8 us (35%)
  waiting for transfers between devices  60.8 us (32%)
  starting transfers between devices  25.1 us (13%)
  local copies, waits for them, and re-layouts  17.3 us (9%)
  other arithmetic  12.6 us (7%)
  matrix products  7.47 us (4%)
    all_gather x1, blocking collectives, on_device(): whole_rows = lax.all_gather(tokens, ('kv', 'tp'), axis=1, tiled=True)  58.2 us
    all_to_all x2, waiting for transfers between devices, summed_on_arrival(): lax.all_to_all(cut_along(shard, dim, length), axis, 0, 0, tiled=True)  31.2 us
    all_to_all x2, waiting for transfers between devices, from_everyone(): lax.all_to_all(jnp.broadcast_to(shard[None], (length, *shard.shape)), axi...  29.6 us
    all_to_all x2, starting transfers between devices, summed_on_arrival(): lax.all_to_all(cut_along(shard, dim, length), axis, 0, 0, tiled=True)  13.6 us
    unnamed x45, local copies, waits for them, and re-layouts  12.9 us
    all_to_all x2, starting transfers between devices, from_everyone(): lax.all_to_all(jnp.broadcast_to(shard[None], (length, *shard.shape)), axi...  11.5 us
    all_to_all x1, blocking collectives, summed_on_arrival(): lax.all_to_all(cut_along(shard, dim, length), axis, 0, 0, tiled=True)  4.89 us
  transfers between devices with their start and end apart: 4, of which 4 were waited for; matrix products, arithmetic and copies ran while one was open for 4% of the time, Pallas kernels for 0%

commit v1 on v0

--- a/solution.py
+++ b/solution.py
@@ -71,7 +71,10 @@
     tp_index = lax.axis_index("tp")
     own_rows = memory.shape[0]
     head_count = memory.shape[1]
-    whole_rows = lax.all_gather(tokens, ("kv", "tp"), axis=1, tiled=True)
+    whole_rows = jnp.concatenate(
+        lax.all_to_all(jnp.stack([tokens] * lax.axis_size(("kv", "tp"))), ("kv", "tp"), 0, 0),
+        axis=1,
+    )
     wide_rows = whole_rows.astype(jnp.float32)
     normed = rms_normed(whole_rows, mix_gain)
     row_span = w_query.shape[0]

time: 192 us -> 173 us (0.901)
  the two profiles are of different devices: /device:TPU:4 before, /device:TPU:2 now
where the time goes in v1:
time: 173 us; the launch traced here: 172 us
  waiting for transfers between devices  83.6 us (48%)
  starting transfers between devices  41.8 us (24%)
  local copies, waits for them, and re-layouts  20.9 us (12%)
  other arithmetic  11.3 us (7%)
  blocking collectives  8.87 us (5%)
  matrix products  4.52 us (3%)
    all_to_all x2, waiting for transfers between devices, summed_on_arrival(): lax.all_to_all(cut_along(shard, dim, length), axis, 0, 0, tiled=True)  32.1 us
    all_to_all x2, waiting for transfers between devices, from_everyone(): lax.all_to_all(jnp.broadcast_to(shard[None], (length, *shard.shape)), axi...  32 us
    all_to_all x1, waiting for transfers between devices, on_device(): lax.all_to_all(jnp.stack([tokens] * lax.axis_size(('kv', 'tp'))), ('kv',...  19.4 us
    all_to_all x1, starting transfers between devices, on_device(): lax.all_to_all(jnp.stack([tokens] * lax.axis_size(('kv', 'tp'))), ('kv',...  17.9 us
    unnamed x51, local copies, waits for them, and re-layouts  16.3 us
    all_to_all x2, starting transfers between devices, from_everyone(): lax.all_to_all(jnp.broadcast_to(shard[None], (length, *shard.shape)), axi...  12 us
    all_to_all x2, starting transfers between devices, summed_on_arrival(): lax.all_to_all(cut_along(shard, dim, length), axis, 0, 0, tiled=True)  11.8 us
    all_to_all x1, blocking collectives, summed_on_arrival(): lax.all_to_all(cut_along(shard, dim, length), axis, 0, 0, tiled=True)  5.02 us
  transfers between devices with their start and end apart: 5, of which 5 were waited for; matrix products, arithmetic and copies ran while one was open for 2% of the time, Pallas kernels for 0%

profile of v1, /device:TPU:2, one launch (start us, length us, event | category | flops | bytes accessed | tf_op | source)
XLA Modules:
  0.0 172.0 jit_solution(4366543810143552614)
XLA Ops:
  0.6 0.0 copy-start
  0.6 0.9 broadcast_bitcast_fusion.1
  1.6 1.4 reshape.287
  3.0 17.9 %all-to-all-start = ((bf16[128,2,1024]{2,1,0:T(2,128)(2,1)}), bf16[128,2,1024]{2,1,0:T(2,128)(2,1)S(1)}, u32[]{:S(2)}, u32[]{:S(2)}) async-start(bf16[128,2,1024]{2,1,0:T(2,128)(2,1)} %reshape.287), calls=%async_computation | async-start | bytes 1048576 | tf_op jit(solution)/shard_map/all_to_all | solution.py:75
  20.9 19.4 %all-to-all-done = bf16[128,2,1024]{2,1,0:T(2,128)(2,1)S(1)} async-done(((bf16[128,2,1024]{2,1,0:T(2,128)(2,1)}), bf16[128,2,1024]{2,1,0:T(2,128)(2,1)S(1)}, u32[]{:S(2)}, u32[]{:S(2)}) %all-to-all-start) | async-done | bytes 524320 | tf_op jit(solution)/shard_map/all_to_all | solution.py:75
  40.3 0.6 reshape.288
  40.9 0.6 multiply_reduce_fusion.1
  41.5 0.0 copy-start.4
  41.5 0.0 copy-start.6
  41.5 1.7 multiply_convert_fusion.1
  43.2 0.3 fusion
  43.5 0.2 fusion.1
  43.7 0.2 fusion.2
  44.0 0.5 broadcast.129
  44.5 1.0 reduce.13
  45.6 1.2 reshape.289
  46.7 5.6 %all-to-all-start.1 = ((bf16[64,2,2048]{2,1,0:T(2,128)(2,1)}), bf16[64,2,2048]{2,1,0:T(2,128)(2,1)}, u32[]{:S(2)}, u32[]{:S(2)}) async-start(bf16[64,2,2048]{2,1,0:T(2,128)(2,1)} %reshape.289), calls=%async_computation.1 | async-start | bytes 1048576 | tf_op jit(solution)/shard_map/all_to_all | solution.py:18
  52.3 0.0 copy-start.1
  52.3 0.7 dynamic-slice_reduce_fusion
  53.1 0.2 fusion.8
  53.3 0.2 bitcast_add_fusion.1
  53.5 0.0 copy-start.10
  53.5 18.2 %all-to-all-done.1 = bf16[64,2,2048]{2,1,0:T(2,128)(2,1)} async-done(((bf16[64,2,2048]{2,1,0:T(2,128)(2,1)}), bf16[64,2,2048]{2,1,0:T(2,128)(2,1)}, u32[]{:S(2)}, u32[]{:S(2)}) %all-to-all-start.1) | async-done | bytes 524320 | tf_op jit(solution)/shard_map/all_to_all | solution.py:18
  71.7 3.6 %reshape.290 = bf16[64,1,4096]{2,1,0:T(2,128)(2,1)S(1)} reshape(bf16[64,2,2048]{2,1,0:T(2,128)(2,1)} %all-to-all-done.1) | data formatting | bytes 1048576
  75.4 1.1 convert_reduce_fusion.1
  76.6 0.0 copy-start.11
  76.6 1.0 fusion.9
  77.5 0.8 multiply_reduce_fusion.3
  78.4 0.1 broadcast_multiply_fusion
  78.5 0.3 broadcast_in_dim.9
  78.8 2.2 %reduce.14 = bf16[64,2048]{1,0:T(8,128)(2,1)S(1)} reduce(bf16[64,1,2048]{2,1,0:T(2,128)(2,1)S(1)} %broadcast_in_dim.9, bf16[]{:T(256)} %broadcast.129), dimensions={1}, to_apply=%broadcast_in_dim.9.reduce_sub_computation | reduce | bytes 524290 | tf_op jit(solution)/shard_map/broadcast_in_dim | solution.py:25
  80.9 0.9 reshape.291
  81.8 6.5 %all-to-all-start.2 = ((bf16[64,2,1024]{2,1,0:T(2,128)(2,1)}), bf16[64,2,1024]{2,1,0:T(2,128)(2,1)S(1)}, u32[]{:S(2)}, u32[]{:S(2)}) async-start(bf16[64,2,1024]{2,1,0:T(2,128)(2,1)} %reshape.291), calls=%async_computation.2 | async-start | bytes 524288 | tf_op jit(solution)/shard_map/all_to_all | solution.py:24
  88.3 0.8 constant_dynamic-slice_fusion
  89.1 0.1 copy.49
  89.2 13.9 %all-to-all-done.2 = bf16[64,2,1024]{2,1,0:T(2,128)(2,1)S(1)} async-done(((bf16[64,2,1024]{2,1,0:T(2,128)(2,1)}), bf16[64,2,1024]{2,1,0:T(2,128)(2,1)S(1)}, u32[]{:S(2)}, u32[]{:S(2)}) %all-to-all-start.2) | async-done | bytes 262176 | tf_op jit(solution)/shard_map/all_to_all | solution.py:24
  103.0 0.2 reshape.292
  103.3 0.3 convolution_convert_fusion.4
  103.6 0.1 reshape.293
  103.7 3.9 %all_to_all.35 = bf16[2,2,2048]{2,1,0:T(2,128)(2,1)S(1)} all-to-all(bf16[2,2,2048]{2,1,0:T(2,128)(2,1)S(1)} %reshape.293), channel_id=1, replica_groups=mesh['dp'=4,'kv'=64,'tp'=2] {'tp'}, dimensions={0} | all-to-all | bytes 32768 | tf_op jit(solution)/shard_map/all_to_all | solution.py:24
  107.6 0.1 reshape.294
  107.7 0.1 copy.39
  107.8 0.3 broadcast_bitcast_fusion
  108.0 1.5 reshape.295
  109.6 5.5 %all-to-all-start.4 = ((bf16[64,2,2048]{2,1,0:T(2,128)(2,1)}), bf16[64,2,2048]{2,1,0:T(2,128)(2,1)}, u32[]{:S(2)}, u32[]{:S(2)}) async-start(bf16[64,2,2048]{2,1,0:T(2,128)(2,1)} %reshape.295), calls=%async_computation.4 | async-start | bytes 1048576 | tf_op jit(solution)/shard_map/all_to_all | solution.py:24
  115.1 0.7 copy.40
  115.8 0.0 copy-start.8
  115.8 0.1 copy.41
  115.9 18.2 %all-to-all-done.4 = bf16[64,2,2048]{2,1,0:T(2,128)(2,1)} async-done(((bf16[64,2,2048]{2,1,0:T(2,128)(2,1)}), bf16[64,2,2048]{2,1,0:T(2,128)(2,1)}, u32[]{:S(2)}, u32[]{:S(2)}) %all-to-all-start.4) | async-done | bytes 524320 | tf_op jit(solution)/shard_map/all_to_all | solution.py:24
  134.0 2.3 %reshape.296 = bf16[64,64,64]{2,1,0:T(8,128)(2,1)S(1)} reshape(bf16[64,2,2048]{2,1,0:T(2,128)(2,1)} %all-to-all-done.4) | data formatting | bytes 1048576
  136.3 0.6 multiply_reduce_fusion
  136.9 2.3 %convolution_convert_fusion = bf16[64,4096]{1,0:T(8,128)(2,1)} fusion(bf16[128,4096]{0,1:T(8,128)(2,1)S(1)} %bitcast.120, bf16[4096,128]{1,0:T(8,128)(2,1)S(1)} %copy-done, bf16[64,4096]{0,1:T(8,128)(2,1)S(1)} %bitcast.117, f32[4096]{0:T(1024)S(1)} %copy-done.8, f32[64]{0:T(128)S(1)} %add_rsqrt_fusion), kind=kOutput, calls=%fused_computation | convolution fusion | flops 135553024 | bytes 3162368 | tf_op jit(solution)/shard_map/dot_general | solution.py:141
  139.2 1.1 copy.60
  140.3 0.0 copy-start.2
  140.3 5.0 %all_to_all.36 = bf16[2,2048,64]{1,2,0:T(8,128)(2,1)} all-to-all(bf16[2,2048,64]{1,2,0:T(8,128)(2,1)S(1)} %bitcast.123), channel_id=1, replica_groups=mesh['dp'=4,'kv'=64,'tp'=2] {'tp'}, dimensions={0} | all-to-all | bytes 1048576 | tf_op jit(solution)/shard_map/all_to_all | solution.py:18
  145.3 1.1 reduce_sum.90
  146.5 1.0 copy.44
  147.5 2.1 %reshape.297 = bf16[64,2,1024]{2,1,0:T(2,128)(2,1)} reshape(bf16[64,32,64]{2,1,0:T(8,128)(2,1)} %bitcast.122) | data formatting | bytes 524288
  149.5 6.2 %all-to-all-start.6 = ((bf16[64,2,1024]{2,1,0:T(2,128)(2,1)}), bf16[64,2,1024]{2,1,0:T(2,128)(2,1)S(1)}, u32[]{:S(2)}, u32[]{:S(2)}) async-start(bf16[64,2,1024]{2,1,0:T(2,128)(2,1)} %reshape.297), calls=%async_computation.6 | async-start | bytes 524288 | tf_op jit(solution)/shard_map/all_to_all | solution.py:18
  155.8 1.3 multiply_add_fusion
  157.1 13.9 %all-to-all-done.6 = bf16[64,2,1024]{2,1,0:T(2,128)(2,1)S(1)} async-done(((bf16[64,2,1024]{2,1,0:T(2,128)(2,1)}), bf16[64,2,1024]{2,1,0:T(2,128)(2,1)S(1)}, u32[]{:S(2)}, u32[]{:S(2)}) %all-to-all-start.6) | async-done | bytes 262176 | tf_op jit(solution)/shard_map/all_to_all | solution.py:18
  171.0 0.3 reshape.298
  171.3 0.1 convert_reduce_fusion
  171.4 0.6 fusion.19
  (40 shorter events, 0.2 us)
Async XLA Ops:
  0.6 136.3 %copy-start = (bf16[4096,128]{1,0:T(8,128)(2,1)S(1)}, bf16[4096,128]{1,0:T(8,128)(2,1)}, u32[]{:S(2)}) copy-start(bf16[4096,128]{1,0:T(8,128)(2,1)} %param.30) | copy-start | bytes 3145732
  3.0 38.5 %copy-start.7 = (f32[4096]{0:T(1024)S(1)}, f32[4096]{0:T(1024)}, u32[]{:S(2)}) copy-start(f32[4096]{0:T(1024)} %param.17) | copy-start | bytes 49156
  3.0 37.4 %all-to-all-start = ((bf16[128,2,1024]{2,1,0:T(2,128)(2,1)}), bf16[128,2,1024]{2,1,0:T(2,128)(2,1)S(1)}, u32[]{:S(2)}, u32[]{:S(2)}) async-start(bf16[128,2,1024]{2,1,0:T(2,128)(2,1)} %reshape.287), calls=%async_computation | async-start | bytes 1048576 | tf_op jit(solution)/shard_map/all_to_all | solution.py:75
  41.5 1.7 copy-start.4
  41.5 2.0 %copy-start.5 = (bf16[64,1024]{1,0:T(8,128)(2,1)S(1)}, bf16[64,1024]{1,0:T(8,128)(2,1)}, u32[]{:S(2)}) copy-start(bf16[64,1024]{1,0:T(8,128)(2,1)} %param.18) | copy-start | bytes 393220
  41.5 2.2 %copy-start.6 = (bf16[64,1024]{1,0:T(8,128)(2,1)S(1)}, bf16[64,1024]{1,0:T(8,128)(2,1)}, u32[]{:S(2)}) copy-start(bf16[64,1024]{1,0:T(8,128)(2,1)} %param.19) | copy-start | bytes 393220
  44.5 8.6 %copy-start.12 = (bf16[4096,16]{0,1:T(8,128)(2,1)S(1)}, bf16[4096,16]{0,1:T(8,128)(2,1)}, u32[]{:S(2)}) copy-start(bf16[4096,16]{0,1:T(8,128)(2,1)} %param.21) | copy-start | bytes 393220
  44.5 8.6 %copy-start.14 = (f32[16]{0:T(128)S(1)}, f32[16]{0:T(128)}, u32[]{:S(2)}) copy-start(f32[16]{0:T(128)} %param.23) | copy-start | bytes 196
  44.5 8.8 %copy-start.13 = (bf16[4096,16]{0,1:T(8,128)(2,1)S(1)}, bf16[4096,16]{0,1:T(8,128)(2,1)}, u32[]{:S(2)}) copy-start(bf16[4096,16]{0,1:T(8,128)(2,1)} %param.22) | copy-start | bytes 393220
  44.5 8.8 %copy-start.15 = (f32[1,8]{1,0:T(1,128)S(1)}, f32[1,8]{1,0:T(1,128)}, u32[]{:S(2)}) copy-start(f32[1,8]{1,0:T(1,128)} %param.27) | copy-start | bytes 100
  44.5 8.8 %copy-start.16 = (f32[16]{0:T(128)S(1)}, f32[16]{0:T(128)}, u32[]{:S(2)}) copy-start(f32[16]{0:T(128)} %param.24) | copy-start | bytes 196
  46.7 25.0 %all-to-all-start.1 = ((bf16[64,2,2048]{2,1,0:T(2,128)(2,1)}), bf16[64,2,2048]{2,1,0:T(2,128)(2,1)}, u32[]{:S(2)}, u32[]{:S(2)}) async-start(bf16[64,2,2048]{2,1,0:T(2,128)(2,1)} %reshape.289), calls=%async_computation.1 | async-start | bytes 1048576 | tf_op jit(solution)/shard_map/all_to_all | solution.py:18
  52.3 24.2 %copy-start.1 = (f32[1,8,256,128]{3,2,1,0:T(8,128)S(1)}, f32[1,8,256,128]{3,2,1,0:T(8,128)}, u32[]{:S(2)}) copy-start(f32[1,8,256,128]{3,2,1,0:T(8,128)} %param.25) | copy-start | bytes 3145732
  53.1 24.5 %copy-start.9 = (f32[1,8,128]{2,1,0:T(8,128)S(1)}, f32[1,8,128]{2,1,0:T(8,128)}, u32[]{:S(2)}) copy-start(f32[1,8,128]{2,1,0:T(8,128)} %param.26) | copy-start | bytes 12292
  53.5 25.3 %copy-start.10 = (f32[1,8]{1,0:T(1,128)}, f32[1,8]{1,0:T(1,128)S(1)}, u32[]{:S(2)}) copy-start(f32[1,8]{1,0:T(1,128)S(1)} %get-tuple-element.7) | copy-start | bytes 100
  76.6 26.7 %copy-start.11 = (bf16[2048,64]{0,1:T(8,128)(2,1)S(1)}, bf16[2048,64]{0,1:T(8,128)(2,1)}, u32[]{:S(2)}) copy-start(bf16[2048,64]{0,1:T(8,128)(2,1)} %param.28) | copy-start | bytes 786436
  81.8 21.2 %all-to-all-start.2 = ((bf16[64,2,1024]{2,1,0:T(2,128)(2,1)}), bf16[64,2,1024]{2,1,0:T(2,128)(2,1)S(1)}, u32[]{:S(2)}, u32[]{:S(2)}) async-start(bf16[64,2,1024]{2,1,0:T(2,128)(2,1)} %reshape.291), calls=%async_computation.2 | async-start | bytes 524288 | tf_op jit(solution)/shard_map/all_to_all | solution.py:24
  103.6 11.5 %copy-start.3 = (bf16[128,4096]{1,0:T(8,128)(2,1)S(1)}, bf16[128,4096]{1,0:T(8,128)(2,1)}, u32[]{:S(2)}) copy-start(bf16[128,4096]{1,0:T(8,128)(2,1)} %param.31) | copy-start | bytes 3145732
  109.6 24.5 %all-to-all-start.4 = ((bf16[64,2,2048]{2,1,0:T(2,128)(2,1)}), bf16[64,2,2048]{2,1,0:T(2,128)(2,1)}, u32[]{:S(2)}, u32[]{:S(2)}) async-start(bf16[64,2,2048]{2,1,0:T(2,128)(2,1)} %reshape.295), calls=%async_computation.4 | async-start | bytes 1048576 | tf_op jit(solution)/shard_map/all_to_all | solution.py:24
  115.8 21.1 %copy-start.8 = (f32[4096]{0:T(1024)S(1)}, f32[4096]{0:T(1024)}, u32[]{:S(2)}) copy-start(f32[4096]{0:T(1024)} %param.29) | copy-start | bytes 49156
  140.3 15.5 %copy-start.2 = (f32[1,8,256,128]{3,2,1,0:T(8,128)S(1)}, f32[1,8,256,128]{3,2,1,0:T(8,128)}, u32[]{:S(2)}) copy-start(f32[1,8,256,128]{3,2,1,0:T(8,128)} %param.25) | copy-start | bytes 3145732
  149.5 21.4 %all-to-all-start.6 = ((bf16[64,2,1024]{2,1,0:T(2,128)(2,1)}), bf16[64,2,1024]{2,1,0:T(2,128)(2,1)S(1)}, u32[]{:S(2)}, u32[]{:S(2)}) async-start(bf16[64,2,1024]{2,1,0:T(2,128)(2,1)} %reshape.297), calls=%async_computation.6 | async-start | bytes 524288 | tf_op jit(solution)/shard_map/all_to_all | solution.py:18
